TPU v7x, 32 devices: a whole 2x2x4 slice. The times are simulated.
32 devices in a mesh: fs: 16 (over z, y, core), tp: 2 (over x).
Axes of the slice: x: 2, y: 2, z: 4, core: 2. Of those that a mesh axis runs over, the one named last changes fastest.
Arguments:
- tokens: bfloat16 [8192, 2048], P('fs', 'tp'), may hold values from -6 to 6
- norm_gain: float32 [2048], P('fs'), may hold values from 0.1 to 1.9
- up_trained: float32 [2048, 4096], P('fs', 'tp'), may hold values from -0.125 to 0.125
- down_trained: float32 [4096, 2048], P('fs', 'tp'), may hold values from -0.09375 to 0.09375
Outputs:
- up_serving: bfloat16 [2048, 4096], P(None, 'tp')
- down_serving: bfloat16 [4096, 2048], P('tp')
- mixed: bfloat16 [8192, 2048], P('fs', 'tp')
All inputs are finite; a program needn't handle non-finite values.
Results may differ from a plain program's by a relative error of at most 0.013.
Values may be sent and summed in bfloat16 or wider, within the bound.
A program may use at most 128 MiB of HBM per device.

v0:
```python
import jax
import jax.numpy as jnp
from jax import lax
from jax.sharding import PartitionSpec as P


def per_device(tokens, norm_gain, up_trained, down_trained):
    up_piece = (norm_gain[:, None] * up_trained).astype(jnp.bfloat16)
    up_serving = lax.all_gather(up_piece, "fs", axis=0, tiled=True)
    down_piece = down_trained.astype(jnp.bfloat16)
    group_count = lax.axis_size("fs")
    pair_count = lax.axis_size("tp")
    sliver = down_piece.shape[1] // group_count
    flipped = down_piece.T
    narrow = lax.all_to_all(flipped, "fs", split_axis=0, concat_axis=1, tiled=True)
    regrouped = lax.all_to_all(narrow, "tp", split_axis=1, concat_axis=0, tiled=True)
    spread = lax.all_gather(regrouped, "fs", axis=0, tiled=True)
    block_width = spread.shape[1]
    ordered = spread.reshape(group_count, pair_count, sliver, block_width).transpose(1, 0, 2, 3)
    down_serving = ordered.reshape(pair_count * group_count * sliver, block_width).T
    features = lax.all_gather(tokens, "tp", axis=1, tiled=True)
    widened = features.astype(jnp.float32)
    scale = lax.rsqrt(jnp.mean(widened * widened, axis=-1, keepdims=True) + 1e-06)
    normed = (widened * scale).astype(jnp.bfloat16)
    preact = jnp.dot(normed, up_serving, preferred_element_type=jnp.float32)
    hidden = jnp.square(jnp.maximum(preact, 0.0)).astype(jnp.bfloat16)
    partial_out = jnp.dot(hidden, down_serving, preferred_element_type=jnp.float32)
    summed = lax.psum_scatter(
        partial_out.astype(jnp.bfloat16), "tp", scatter_dimension=1, tiled=True
    )
    return (up_serving, down_serving, summed)


def solution(mesh):
    placed = (P("fs", "tp"), P("fs"), P("fs", "tp"), P("fs", "tp"))
    return jax.shard_map(
        per_device,
        mesh=mesh,
        in_specs=placed,
        out_specs=(P(None, "tp"), P("tp", None), P("fs", "tp")),
        check_vma=False,
    )
```

profile of v0, /device:TPU:0, one launch (start us, length us, event | category | flops | bytes accessed | tf_op | source)
XLA Modules:
  0.0 264.8 jit_solution(10153047460143289739)
XLA Ops:
  7.2 0.0 all-gather.8.cloned.1.call-start
  7.2 0.7 all-gather.8.cloned.1.call-update
  7.9 0.0 all-gather.6.cloned.1.call-start
  8.0 1.4 copy.12
  9.4 21.5 %all_to_all.35 = bf16[16,64,256]{2,1,0:T(8,128)(2,1)S(1)} all-to-all(bf16[16,64,256]{2,1,0:T(8,128)(2,1)S(1)} %bitcast.23), channel_id=1, replica_groups=mesh['fs'=16,'tp'=2] {'fs'}, dimensions={0} | all-to-all | bytes 1048576 | tf_op jit(solution)/shard_map/all_to_all | solution.py:15
  30.9 0.3 copy.13
  31.2 0.1 all_to_all.29
  31.3 0.2 copy.14
  31.5 17.9 %all_to_all.36 = bf16[64,2,2048]{2,0,1:T(8,128)(2,1)} all-to-all(bf16[64,2,2048]{2,0,1:T(8,128)(2,1)S(1)} %copy.14), channel_id=1, replica_groups=mesh['fs'=16,'tp'=2] {'tp'}, dimensions={1} | all-to-all | bytes 1048576 | tf_op jit(solution)/shard_map/all_to_all | solution.py:16
  49.4 0.0 all-gather.6.cloned.1.call-update
  49.4 0.0 all-gather.4.cloned.1.call-start
  49.5 0.9 multiply_convert_fusion.1
  50.4 0.0 all-gather.4.cloned.1.call-update
  50.4 0.0 reduce-scatter.2.cloned.1.call-start
  50.5 0.6 all-gather.8.cloned.1.call-done
  51.0 2.1 fusion
  53.1 74.4 %all-gather.6.cloned.1.call-done = bf16[2048,2048]{1,0:T(8,128)(2,1)} async-done(((bf16[128,2048]{1,0:T(8,128)(2,1)}), bf16[2048,2048]{1,0:T(8,128)(2,1)}) %all-gather.6.cloned.1.call-update) | async-done | bytes 8388624 | tf_op jit(solution)/shard_map/all_gather | solution.py:17
  127.5 8.6 %copy.15 = bf16[2,16,64,2048]{3,2,1,0:T(8,128)(2,1)} copy(bf16[2,16,64,2048]{3,2,0,1:T(8,128)(2,1)} %bitcast.22) | data formatting | bytes 16777216 | tf_op jit(solution)/shard_map/transpose | solution.py:19
  136.1 67.1 %all-gather.4.cloned.1.call-done = bf16[2048,2048]{1,0:T(8,128)(2,1)} async-done(((bf16[128,2048]{1,0:T(8,128)(2,1)}), bf16[2048,2048]{1,0:T(8,128)(2,1)}) %all-gather.4.cloned.1.call-update) | async-done | bytes 8388624 | tf_op jit(solution)/shard_map/all_gather | solution.py:9
  203.2 16.0 %convolution_convert_fusion = bf16[512,2048]{1,0:T(8,128)(2,1)} fusion(bf16[2048,2048]{1,0:T(8,128)(2,1)} %bitcast.20, bf16[2048,2048]{1,0:T(8,128)(2,1)} %all-gather.4.cloned.1.call-done, bf16[512,2048]{1,0:T(8,128)(2,1)S(1)} %copy-done, f32[512]{0:T(512)S(1)} %add_rsqrt_fusion), kind=kOutput, calls=%fused_computation.5 | convolution fusion | flops 8597274624 | bytes 20973568 | tf_op jit(solution)/shard_map/dot_general | solution.py:27
  219.1 0.0 reduce-scatter.2.cloned.1.call-update
  219.2 11.9 %copy.16 = bf16[2048,2048]{1,0:T(8,128)(2,1)} copy(bf16[2048,2048]{0,1:T(8,128)(2,1)} %bitcast.21) | data formatting | bytes 16777216
  231.1 18.7 %reduce-scatter.2.cloned.1.call-done = bf16[512,1024]{1,0:T(8,128)(2,1)} async-done(((bf16[512,2048]{1,0:T(8,128)(2,1)}), bf16[512,1024]{1,0:T(8,128)(2,1)}) %reduce-scatter.2.cloned.1.call-update) | async-done | bytes 1048592 | tf_op jit(solution)/shard_map/reduce_scatter | solution.py:28
  249.8 8.4 %copy.18 = bf16[2048,2048]{1,0:T(8,128)(2,1)} copy(bf16[2048,2048]{1,0:T(8,128)(2,1)} %all-gather.4.cloned.1.call-done) | data formatting | bytes 16777216
  (7 shorter events, 0.0 us)
Async XLA Ops:
  7.2 42.3 %copy-start.2 = (f32[128]{0:T(128)S(1)}, f32[128]{0:T(128)}, u32[]{:S(2)}) copy-start(f32[128]{0:T(128)} %param.5) | copy-start | bytes 1540
  7.2 42.3 %copy-start.1 = (f32[128,2048]{1,0:T(8,128)S(1)}, f32[128,2048]{1,0:T(8,128)}, u32[]{:S(2)}) copy-start(f32[128,2048]{1,0:T(8,128)} %param.6) | copy-start | bytes 3145732
  7.2 43.8 %all-gather.8.cloned.1.call-start = ((), (), s32[]{:S(2)}) async-start(), calls=%async_computation.5 | async-start | bytes 3145728 | tf_op jit(solution)/shard_map/all_gather | solution.py:21
  7.9 119.6 %all-gather.6.cloned.1.call-start = ((), (), s32[]{:S(2)}) async-start(), calls=%async_computation.4 | async-start | bytes 8912896 | tf_op jit(solution)/shard_map/all_gather | solution.py:17
  49.4 153.8 %all-gather.4.cloned.1.call-start = ((), (), s32[]{:S(2)}) async-start(), calls=%async_computation.3 | async-start | bytes 8912896 | tf_op jit(solution)/shard_map/all_gather | solution.py:9
  50.4 199.4 %reduce-scatter.2.cloned.1.call-start = ((), (), s32[]{:S(2)}) async-start(), calls=%async_computation.6 | async-start | bytes 3145728 | tf_op jit(solution)/shard_map/reduce_scatter | solution.py:28
  127.5 75.7 %copy-start = (bf16[512,2048]{1,0:T(8,128)(2,1)S(1)}, bf16[512,2048]{1,0:T(8,128)(2,1)}, u32[]{:S(2)}) copy-start(bf16[512,2048]{1,0:T(8,128)(2,1)} %all-gather.8.cloned.1.call-done) | copy-start | bytes 6291460
Sparse Core Ops, SparseCore 0:
  9.5 41.4 all-gather.7
  53.2 74.2 all-gather.5
  130.2 72.8 all-gather.3
  219.3 30.4 reduce-scatter.1
where the time goes:
time: 265 us
  waiting for transfers between devices  161 us (61%)
  blocking collectives  39.4 us (15%)
  local copies, waits for them, and re-layouts  31 us (12%)
  matrix products  16 us (6%)
  between operations  13.8 us (5%)
  other arithmetic  3 us (1%)
    all_gather x1, waiting for transfers between devices, per_device(): spread = lax.all_gather(regrouped, 'fs', axis=0, tiled=True)  74.4 us
    all_gather x1, waiting for transfers between devices, per_device(): up_serving = lax.all_gather(up_piece, 'fs', axis=0, tiled=True)  67.1 us
    unnamed x9, local copies, waits for them, and re-layouts  21.8 us
    all_to_all x1, blocking collectives, per_device(): lax.all_to_all(flipped, 'fs', split_axis=0, concat_axis=1, tiled=True)  21.5 us
    reduce_scatter x1, waiting for transfers between devices, per_device(): lax.psum_scatter(partial_out.astype(jnp.bfloat16), 'tp', scatter_dimensio...  18.7 us
    all_to_all x1, blocking collectives, per_device(): lax.all_to_all(narrow, 'tp', split_axis=1, concat_axis=0, tiled=True)  17.9 us
    dot_general x1, matrix products, per_device(): jnp.dot(hidden, down_serving, preferred_element_type=jnp.float32)  16 us
    transpose x1, local copies, waits for them, and re-layouts, per_device(): spread.reshape(group_count, pair_count, sliver, block_width)  8.59 us
  transfers between devices with their start and end apart: 4, of which 4 were waited for; matrix products, arithmetic and copies ran while one was open for 10% of the time, Pallas kernels for 0%

commit v1 on v0

--- a/solution.py
+++ b/solution.py
@@ -14,7 +14,9 @@
     flipped = down_piece.T
     narrow = lax.all_to_all(flipped, "fs", split_axis=0, concat_axis=1, tiled=True)
     regrouped = lax.all_to_all(narrow, "tp", split_axis=1, concat_axis=0, tiled=True)
-    spread = lax.all_gather(regrouped, "fs", axis=0, tiled=True)
+    spread = jnp.concatenate(
+        lax.all_to_all(jnp.stack([regrouped] * lax.axis_size("fs")), "fs", 0, 0), axis=0
+    )
     block_width = spread.shape[1]
     ordered = spread.reshape(group_count, pair_count, sliver, block_width).transpose(1, 0, 2, 3)
     down_serving = ordered.reshape(pair_count * group_count * sliver, block_width).T

time: 265 us -> 362 us (1.37)
  waiting for transfers between devices: 161 us -> 249 us
  starting transfers between devices: 0.16 us -> 5.04 us
  local copies, waits for them, and re-layouts: 31 us -> 35.7 us
    all_to_all x0 -> x1, waiting for transfers between devices: none -> 198 us  [per_device(): lax.all_to_all(jnp.stack([regrouped] * lax.axis_size('fs')), 'fs', 0, 0)]
    all_gather x1 -> x0, waiting for transfers between devices: 74.4 us -> none  [per_device(): spread = lax.all_gather(regrouped, 'fs', axis=0, tiled=True)]
    all_gather x1, waiting for transfers between devices: 67.1 us -> 0.01 us  [per_device(): up_serving = lax.all_gather(up_piece, 'fs', axis=0, tiled=True)]
    reduce_scatter x1, waiting for transfers between devices: 18.7 us -> 50.7 us  [per_device(): lax.psum_scatter(partial_out.astype(jnp.bfloat16), 'tp', scatter_dimensio...]
    all_to_all x0 -> x1, starting transfers between devices: none -> 4.91 us  [per_device(): lax.all_to_all(jnp.stack([regrouped] * lax.axis_size('fs')), 'fs', 0, 0)]
    another operation x0 -> x1, local copies, waits for them, and re-layouts: none -> 4.47 us  [per_device(): jnp.stack([regrouped] * lax.axis_size('fs'))]
  transfers between devices with their start and end apart: 4 -> 4, of which waited for: 4 -> 2; matrix products, arithmetic and copies ran while one was open for 10% -> 8% of each run, Pallas kernels for 0% -> 0%
where the time goes in v1:
time: 362 us
  waiting for transfers between devices  249 us (69%)
  blocking collectives  38.8 us (11%)
  local copies, waits for them, and re-layouts  35.7 us (10%)
  matrix products  16 us (4%)
  between operations  13.8 us (4%)
  starting transfers between devices  5.04 us (1%)
    all_to_all x1, waiting for transfers between devices, per_device(): lax.all_to_all(jnp.stack([regrouped] * lax.axis_size('fs')), 'fs', 0, 0)  198 us
    reduce_scatter x1, waiting for transfers between devices, per_device(): lax.psum_scatter(partial_out.astype(jnp.bfloat16), 'tp', scatter_dimensio...  50.7 us
    unnamed x9, local copies, waits for them, and re-layouts  22.1 us
    all_to_all x1, blocking collectives, per_device(): lax.all_to_all(flipped, 'fs', split_axis=0, concat_axis=1, tiled=True)  21.5 us
    all_to_all x1, blocking collectives, per_device(): lax.all_to_all(narrow, 'tp', split_axis=1, concat_axis=0, tiled=True)  17.3 us
    dot_general x1, matrix products, per_device(): jnp.dot(hidden, down_serving, preferred_element_type=jnp.float32)  16 us
    transpose x1, local copies, waits for them, and re-layouts, per_device(): spread.reshape(group_count, pair_count, sliver, block_width)  8.59 us
  transfers between devices with their start and end apart: 4, of which 2 were waited for; matrix products, arithmetic and copies ran while one was open for 8% of the time, Pallas kernels for 0%

profile of v1, /device:TPU:0, one launch (start us, length us, event | category | flops | bytes accessed | tf_op | source)
XLA Modules:
  0.0 361.6 jit_solution(6687419041700266155)
XLA Ops:
  7.2 0.0 all-gather.5.cloned.1.call-start
  7.2 0.7 all-gather.5.cloned.1.call-update
  7.9 1.4 copy.12
  9.3 21.5 %all_to_all.37 = bf16[16,64,256]{2,1,0:T(8,128)(2,1)S(1)} all-to-all(bf16[16,64,256]{2,1,0:T(8,128)(2,1)S(1)} %bitcast.23), channel_id=1, replica_groups=mesh['fs'=16,'tp'=2] {'fs'}, dimensions={0} | all-to-all | bytes 1048576 | tf_op jit(solution)/shard_map/all_to_all | solution.py:15
  30.8 0.3 copy.13
  31.1 0.1 all_to_all.30
  31.2 0.2 copy.14
  31.4 17.3 %all_to_all.38 = bf16[64,2,2048]{2,0,1:T(8,128)(2,1)S(1)} all-to-all(bf16[64,2,2048]{2,0,1:T(8,128)(2,1)S(1)} %copy.14), channel_id=1, replica_groups=mesh['fs'=16,'tp'=2] {'tp'}, dimensions={1} | all-to-all | bytes 1048576 | tf_op jit(solution)/shard_map/all_to_all | solution.py:16
  48.7 4.5 %stack.5 = bf16[16,128,2048]{2,1,0:T(8,128)(2,1)} broadcast(bf16[128,2048]{1,0:T(8,128)(2,1)S(1)} %bitcast.22), dimensions={1,2} | broadcast | bytes 8912896 | tf_op jit(solution)/shard_map/stack | solution.py:18
  53.2 4.9 %all-to-all-start.2 = ((bf16[16,128,2048]{2,1,0:T(8,128)(2,1)}), bf16[16,128,2048]{2,1,0:T(8,128)(2,1)}, u32[]{:S(2)}, u32[]{:S(2)}) async-start(bf16[16,128,2048]{2,1,0:T(8,128)(2,1)} %stack.5), calls=%async_computation.2 | async-start | bytes 16777216 | tf_op jit(solution)/shard_map/all_to_all | solution.py:18
  58.1 0.0 all-gather.3.cloned.1.call-start
  58.1 0.0 copy-done.1
  58.1 0.9 multiply_convert_fusion.1
  59.1 0.0 all-gather.3.cloned.1.call-update
  59.1 0.0 reduce-scatter.2.cloned.1.call-start
  59.1 0.0 all-gather.5.cloned.1.call-done
  59.2 2.1 fusion
  61.2 197.9 %all-to-all-done.2 = bf16[16,128,2048]{2,1,0:T(8,128)(2,1)} async-done(((bf16[16,128,2048]{2,1,0:T(8,128)(2,1)}), bf16[16,128,2048]{2,1,0:T(8,128)(2,1)}, u32[]{:S(2)}, u32[]{:S(2)}) %all-to-all-start.2) | async-done | bytes 8388640 | tf_op jit(solution)/shard_map/all_to_all | solution.py:18
  259.1 8.6 %copy.15 = bf16[2,16,64,2048]{3,2,1,0:T(8,128)(2,1)} copy(bf16[2,16,64,2048]{3,2,0,1:T(8,128)(2,1)} %bitcast.6) | data formatting | bytes 16777216 | tf_op jit(solution)/shard_map/transpose | solution.py:21
  267.7 16.0 %convolution_convert_fusion = bf16[512,2048]{1,0:T(8,128)(2,1)} fusion(bf16[2048,2048]{1,0:T(8,128)(2,1)} %bitcast.20, bf16[2048,2048]{1,0:T(8,128)(2,1)} %all-gather.3.cloned.1.call-done, bf16[512,2048]{1,0:T(8,128)(2,1)S(1)} %copy-done, f32[512]{0:T(512)S(1)} %add_rsqrt_fusion), kind=kOutput, calls=%fused_computation.5 | convolution fusion | flops 8597274624 | bytes 20973568 | tf_op jit(solution)/shard_map/dot_general | solution.py:29
  283.7 0.0 reduce-scatter.2.cloned.1.call-update
  283.8 12.2 %copy.16 = bf16[2048,2048]{1,0:T(8,128)(2,1)} copy(bf16[2048,2048]{0,1:T(8,128)(2,1)} %bitcast.21) | data formatting | bytes 16777216
  296.0 50.7 %reduce-scatter.2.cloned.1.call-done = bf16[512,1024]{1,0:T(8,128)(2,1)} async-done(((bf16[512,2048]{1,0:T(8,128)(2,1)}), bf16[512,1024]{1,0:T(8,128)(2,1)}) %reduce-scatter.2.cloned.1.call-update) | async-done | bytes 1048592 | tf_op jit(solution)/shard_map/reduce_scatter | solution.py:30
  346.7 8.4 %copy.18 = bf16[2048,2048]{1,0:T(8,128)(2,1)} copy(bf16[2048,2048]{1,0:T(8,128)(2,1)} %all-gather.3.cloned.1.call-done) | data formatting | bytes 16777216
  (7 shorter events, 0.0 us)
Async XLA Ops:
  7.2 52.0 %all-gather.5.cloned.1.call-start = ((), (), s32[]{:S(2)}) async-start(), calls=%async_computation.5 | async-start | bytes 3145728 | tf_op jit(solution)/shard_map/all_gather | solution.py:23
  53.1 5.0 %copy-start.1 = (f32[128,2048]{1,0:T(8,128)S(1)}, f32[128,2048]{1,0:T(8,128)}, u32[]{:S(2)}) copy-start(f32[128,2048]{1,0:T(8,128)} %param.6) | copy-start | bytes 3145732
  53.2 5.0 %copy-start.2 = (f32[128]{0:T(128)S(1)}, f32[128]{0:T(128)}, u32[]{:S(2)}) copy-start(f32[128]{0:T(128)} %param.5) | copy-start | bytes 1540
  53.2 206.0 %all-to-all-start.2 = ((bf16[16,128,2048]{2,1,0:T(8,128)(2,1)}), bf16[16,128,2048]{2,1,0:T(8,128)(2,1)}, u32[]{:S(2)}, u32[]{:S(2)}) async-start(bf16[16,128,2048]{2,1,0:T(8,128)(2,1)} %stack.5), calls=%async_computation.2 | async-start | bytes 16777216 | tf_op jit(solution)/shard_map/all_to_all | solution.py:18
  58.1 209.7 %all-gather.3.cloned.1.call-start = ((), (), s32[]{:S(2)}) async-start(), calls=%async_computation.4 | async-start | bytes 8912896 | tf_op jit(solution)/shard_map/all_gather | solution.py:9
  59.1 287.6 %reduce-scatter.2.cloned.1.call-start = ((), (), s32[]{:S(2)}) async-start(), calls=%async_computation.6 | async-start | bytes 3145728 | tf_op jit(solution)/shard_map/reduce_scatter | solution.py:30
  259.1 8.6 %copy-start = (bf16[512,2048]{1,0:T(8,128)(2,1)S(1)}, bf16[512,2048]{1,0:T(8,128)(2,1)}, u32[]{:S(2)}) copy-start(bf16[512,2048]{1,0:T(8,128)(2,1)} %all-gather.5.cloned.1.call-done) | copy-start | bytes 6291460
Sparse Core Ops, SparseCore 0:
  9.5 41.4 all-gather.4
  61.6 183.0 all-gather.2
  283.9 62.7 reduce-scatter.1
